TPU v7x, 32 devices: a whole 2x2x4 slice. The times are simulated.
32 devices in a mesh: ep: 8 (over z, y), tp: 4 (over x, core).
Axes of the slice: x: 2, y: 2, z: 4, core: 2. Of those that a mesh axis runs over, the one named last changes fastest.
Arguments:
- mixer_in: bfloat16 [4096, 4096], P(('ep', 'tp')), may hold values from -6 to 6
- mixer_gain: float32 [4096], replicated, may hold values from 0.1 to 1.9
- group_weight: bfloat16 [4, 1024, 1024], P('tp'), may hold values from -0.1875 to 0.1875
- group_scale: float32 [4, 1024], P('tp'), may hold values from 0.1 to 1.9
- expert_in: bfloat16 [4096, 4096], P(('ep', 'tp')), may hold values from -6 to 6
- expert_gain: float32 [4096], replicated, may hold values from 0.1 to 1.9
- routes: int32 [4096, 2], P('ep'), may hold values from 0 to 7, all different within a row; in each aligned block of 128 rows (0 to 127, 128 to 255, ...) at most 48 rows name the same one
- route_weight: float32 [4096, 2], P('ep'), may hold values from 0.2 to 1
- gate_weight: bfloat16 [8, 4096, 1024], P('ep', None, 'tp'), may hold values from -0.25 to 0.25
- up_weight: bfloat16 [8, 4096, 1024], P('ep', None, 'tp'), may hold values from -0.25 to 0.25
- down_weight: bfloat16 [8, 1024, 4096], P('ep', 'tp'), may hold values from -0.02734375 to 0.02734375
Outputs:
- mixed: bfloat16 [4096, 4096], P('ep', 'tp')
- expert_out: bfloat16 [4096, 4096], P(('ep', 'tp'))
Inputs may be any that keep to these rules, and one draw needn't show every extreme that they name: `routes`: each row names 2 different experts; within the rows of one device (aligned blocks of 128 rows) no expert is named more than 48 times, and that count is reached.
All inputs are finite; a program needn't handle non-finite values.
Results may differ from a plain program's by a relative error of at most 0.012.
Values may be sent and summed in bfloat16 or wider, within the bound.
A program may use at most 128 MiB of HBM per device.

v0:
```python
import jax
import jax.numpy as jnp
from jax import lax
from jax.sharding import PartitionSpec as P

WMAX = 16
TOP = 2


epsilon = 1e-06
clamp_limit = 7.0
sigmoid_slope = 1.702


def from_behind(x, axis, by):
    count = lax.axis_size(axis)
    pairs = [(i, i + by) for i in range(count) if 0 <= i + by < count]
    return lax.ppermute(x, axis, pairs)


def rms_norm(values, gain):
    widened = values.astype(jnp.float32)
    scaled = widened * lax.rsqrt(jnp.mean(widened * widened, axis=-1, keepdims=True) + epsilon)
    return (scaled * gain).astype(jnp.bfloat16)


def clamped_unit(gate_part, up_part):
    gate_part = jnp.minimum(gate_part, clamp_limit)
    up_part = jnp.clip(up_part, -clamp_limit, clamp_limit)
    return ((up_part + 1.0) * gate_part * jax.nn.sigmoid(sigmoid_slope * gate_part)).astype(
        jnp.bfloat16
    )


def slot_table(block_routes, experts, capacity):
    count = block_routes.shape[0]
    onehot = (
        block_routes[:, :, None] == jnp.arange(experts, dtype=jnp.int32)[None, None, :]
    ).astype(jnp.int32)
    per_token = jnp.sum(onehot, axis=1)
    earlier = jnp.cumsum(per_token, axis=0) - per_token
    slot_rank = jnp.sum(onehot * earlier[:, None, :], axis=2)
    matches = onehot[:, :, :, None] * (
        slot_rank[:, :, None, None] == jnp.arange(capacity, dtype=jnp.int32)[None, None, None, :]
    ).astype(jnp.int32)
    source = jnp.sum(matches * jnp.arange(count, dtype=jnp.int32)[:, None, None, None], axis=(0, 1))
    filled = jnp.sum(matches, axis=(0, 1))
    return (source, filled, slot_rank)


def shards(
    mixer_in,
    mixer_gain,
    group_weight,
    group_scale,
    expert_in,
    expert_gain,
    routes,
    route_weight,
    gate_weight,
    up_weight,
    down_weight,
):
    normed = rms_norm(mixer_in, mixer_gain)
    shard_rows = lax.all_to_all(normed, "tp", split_axis=1, concat_axis=0, tiled=True)
    length = shard_rows.shape[0]
    last_rows = shard_rows[length - (WMAX - 1) :]
    before = from_behind(last_rows, "ep", 1)
    extended = jnp.concatenate([before, shard_rows], axis=0).astype(jnp.float32)
    window = 2 << lax.axis_index("tp")
    position = lax.axis_index("ep") * length + jnp.arange(length, dtype=jnp.int32)
    prefix = jnp.concatenate(
        [jnp.zeros((1, extended.shape[1]), jnp.float32), jnp.cumsum(extended, axis=0)], axis=0
    )
    upper = prefix[WMAX:]
    lower = lax.dynamic_slice_in_dim(prefix, WMAX - window, length, 0)
    counts = jnp.minimum(position + 1, window).astype(jnp.float32)[:, None]
    pooled = ((upper - lower) / counts - extended[WMAX - 1 :]).astype(jnp.bfloat16)
    mixed = (
        jnp.dot(pooled, group_weight[0], preferred_element_type=jnp.float32) * group_scale[0]
    ).astype(jnp.bfloat16)
    expert_norm = rms_norm(expert_in, expert_gain)
    tok_count = expert_in.shape[0]
    width = expert_in.shape[1]
    experts = lax.axis_size("ep")
    capacity = max(2, 3 * tok_count * TOP // (2 * experts))
    tp_index = lax.axis_index("tp")
    own_routes = lax.dynamic_slice_in_dim(routes, tp_index * tok_count, tok_count, 0)
    own_weight = lax.dynamic_slice_in_dim(route_weight, tp_index * tok_count, tok_count, 0)
    gate_local = gate_weight[0]
    up_local = up_weight[0]
    source, filled, own_rank = slot_table(own_routes, experts, capacity)
    outgoing = expert_norm[source] * filled[:, :, None].astype(jnp.bfloat16)
    arrived = lax.all_to_all(outgoing, "ep", split_axis=0, concat_axis=0, tiled=True)
    piece = lax.all_gather(arrived.reshape(-1, width), "tp", axis=0, tiled=True)
    hidden = clamped_unit(
        jnp.dot(piece, gate_local, preferred_element_type=jnp.float32),
        jnp.dot(piece, up_local, preferred_element_type=jnp.float32),
    )
    down_local = down_weight[0]
    summed = lax.psum_scatter(
        jnp.dot(hidden, down_local, preferred_element_type=jnp.float32).astype(jnp.bfloat16),
        "tp",
        scatter_dimension=0,
        tiled=True,
    ).astype(jnp.float32)
    summed = summed.astype(jnp.bfloat16).reshape(experts, capacity, width)
    returned = lax.all_to_all(summed, "ep", split_axis=0, concat_axis=0, tiled=True)
    flat_rows = returned.reshape(-1, width)
    slot_index = own_routes * capacity + own_rank
    expert_sum = jnp.zeros((tok_count, width), jnp.float32)
    for choice_slot in range(TOP):
        expert_sum = (
            expert_sum
            + flat_rows[slot_index[:, choice_slot]].astype(jnp.float32)
            * own_weight[:, choice_slot : choice_slot + 1]
        )
    return (mixed, expert_sum.astype(jnp.bfloat16))


def solution(mesh):
    in_specs = (
        P(("ep", "tp"), None),
        P(),
        P("tp", None, None),
        P("tp", None),
        P(("ep", "tp"), None),
        P(),
        P("ep", None),
        P("ep", None),
        P("ep", None, "tp"),
        P("ep", None, "tp"),
        P("ep", "tp", None),
    )
    out_specs = (P("ep", "tp"), P(("ep", "tp"), None))
    return jax.shard_map(shards, mesh=mesh, in_specs=in_specs, out_specs=out_specs, check_vma=False)
```

profile of v0, /device:TPU:17, one launch (start us, length us, event | category | flops | bytes accessed | tf_op | source)
XLA Modules:
  0.0 413.8 jit_solution(10830611905956360043)
XLA Ops:
  7.2 0.0 copy-start
  7.2 0.0 all-gather.2.cloned.1.call-start
  7.2 0.8 constant_dynamic-slice_fusion.1
  8.1 0.1 copy.29
  8.2 0.2 reduce_window_sum.28
  8.4 0.4 multiply_reduce_fusion
  8.8 0.1 reshape.99
  8.9 1.5 fusion.12
  10.5 1.6 fusion.14
  12.0 4.0 gather_fusion
  16.1 2.2 broadcast_multiply_fusion
  18.2 74.2 %all_to_all.29 = bf16[8,48,4096]{2,1,0:T(8,128)(2,1)} all-to-all(bf16[8,48,4096]{2,1,0:T(8,128)(2,1)S(1)} %broadcast_multiply_fusion), channel_id=1, replica_groups=mesh['ep'=8,'tp'=4] {'ep'}, dimensions={0} | all-to-all | bytes 6291456 | tf_op jit(solution)/shard_map/all_to_all | solution.py:94
  92.4 0.0 all-gather.2.cloned.1.call-update
  92.4 0.2 reduce-scatter.2.cloned.1.call-start
  92.6 83.5 %all-gather.2.cloned.1.call-done = bf16[1536,4096]{1,0:T(8,128)(2,1)} async-done(((bf16[384,4096]{1,0:T(8,128)(2,1)}), bf16[1536,4096]{1,0:T(8,128)(2,1)}) %all-gather.2.cloned.1.call-update) | async-done | bytes 12582928 | tf_op jit(solution)/shard_map/all_gather | solution.py:95
  176.2 9.9 %convolution_minimum_fusion = f32[1536,256]{1,0:T(8,128)} fusion(bf16[1536,4096]{1,0:T(8,128)(2,1)} %all-gather.2.cloned.1.call-done, bf16[1,4096,256]{2,1,0:T(8,128)(2,1)} %param.19), kind=kOutput, calls=%fused_computation.6 | convolution fusion | flops 3221618688 | bytes 16252928 | tf_op jit(solution)/shard_map/dot_general | solution.py:97
  186.0 19.5 %convolution_convert_fusion = bf16[1536,4096]{1,0:T(8,128)(2,1)} fusion(f32[1536,256]{1,0:T(8,128)} %convolution_minimum_fusion, bf16[1536,4096]{1,0:T(8,128)(2,1)} %all-gather.2.cloned.1.call-done, bf16[1,256,4096]{2,1,0:T(8,128)(2,1)S(1)} %copy-done, bf16[1,4096,256]{2,1,0:T(8,128)(2,1)} %param.20), kind=kOutput, calls=%fused_computation.3 | convolution fusion | flops 6452281344 | bytes 30932992 | tf_op jit(solution)/shard_map/dot_general | solution.py:102
  205.5 0.0 reduce-scatter.2.cloned.1.call-update
  205.5 1.2 copy-done.4
  206.7 0.7 copy.25
  207.4 0.6 fusion.9
  208.0 0.7 fusion.11
  208.7 16.1 %all_to_all.30 = bf16[128,4,1024]{0,2,1:T(8,128)(2,1)S(1)} all-to-all(bf16[128,4,1024]{0,2,1:T(8,128)(2,1)S(1)} %bitcast.53), channel_id=1, replica_groups=mesh['ep'=8,'tp'=4] {'tp'}, dimensions={1} | all-to-all | bytes 2097152 | tf_op jit(solution)/shard_map/all_to_all | solution.py:65
  224.7 77.7 %reduce-scatter.2.cloned.1.call-done = bf16[384,4096]{1,0:T(8,128)(2,1)} async-done(((bf16[1536,4096]{1,0:T(8,128)(2,1)}), bf16[384,4096]{1,0:T(8,128)(2,1)}) %reduce-scatter.2.cloned.1.call-update) | async-done | bytes 3145744 | tf_op jit(solution)/shard_map/reduce_scatter | solution.py:101
  302.5 5.5 %all-to-all-start.2 = ((bf16[8,48,4096]{2,1,0:T(8,128)(2,1)}), bf16[8,48,4096]{2,1,0:T(8,128)(2,1)}, u32[]{:S(2)}, u32[]{:S(2)}) async-start(bf16[8,48,4096]{2,1,0:T(8,128)(2,1)} %bitcast.55), calls=%async_computation.3 | async-start | bytes 6291456 | tf_op jit(solution)/shard_map/all_to_all | solution.py:108
  307.9 0.7 constant_dynamic-slice_fusion
  308.6 0.7 multiply_add_fusion
  309.3 0.5 copy.26
  309.9 3.3 collective-permute-start
  313.2 65.4 %collective-permute-done = bf16[15,1024]{1,0:T(8,128)(2,1)S(1)} collective-permute-done((bf16[15,1024]{1,0:T(8,128)(2,1)S(1)}, bf16[15,1024]{1,0:T(8,128)(2,1)S(1)}, u32[]{:S(2)}, u32[]{:S(2)}) %collective-permute-start) | collective-permute-done | bytes 30752 | tf_op jit(solution)/shard_map/ppermute | solution.py:18
  378.6 1.6 fusion.36
  380.3 0.3 pad.4
  380.6 2.6 fusion
  383.2 0.0 copy-start.2
  383.2 1.9 copy-done.2
  385.1 2.6 broadcast_add_fusion
  387.8 1.5 copy.28
  389.3 0.0 copy-start.6
  389.3 0.0 copy-start.7
  389.3 0.2 slice.51
  389.6 1.3 copy-done.3
  390.9 0.6 copy-done.6
  391.5 2.6 multiply_convert_fusion
  394.1 0.0 all-to-all-done.2
  394.1 4.5 %gather_fusion.1 = bf16[128,4096]{1,0:T(8,128)(2,1)S(1)} fusion(bf16[384,4096]{1,0:T(8,128)(2,1)} %bitcast.18, s32[1024]{0:T(1024)S(1)} %get-tuple-element.11), kind=kCustom, calls=%fused_computation.1 | custom fusion | bytes 2097664 | tf_op jit(solution)/shard_map/gather | solution.py:115
  398.6 0.0 copy-start.1
  398.6 5.6 %gather_fusion.2 = bf16[128,4096]{1,0:T(8,128)(2,1)} fusion(bf16[384,4096]{1,0:T(8,128)(2,1)} %bitcast.18, s32[1024]{0:T(1024)S(1)} %get-tuple-element.10), kind=kCustom, calls=%fused_computation.2 | custom fusion | bytes 2097664 | tf_op jit(solution)/shard_map/gather | solution.py:115
  404.3 2.7 add_convert_fusion
  (25 shorter events, 0.2 us)
Async XLA Ops:
  7.2 178.9 %copy-start = (bf16[1,256,4096]{2,1,0:T(8,128)(2,1)S(1)}, bf16[1,256,4096]{2,1,0:T(8,128)(2,1)}, u32[]{:S(2)}) copy-start(bf16[1,256,4096]{2,1,0:T(8,128)(2,1)} %param.21) | copy-start | bytes 6291460
  7.2 169.0 %all-gather.2.cloned.1.call-start = ((), (), s32[]{:S(2)}) async-start(), calls=%async_computation.4 | async-start | bytes 15728640 | tf_op jit(solution)/shard_map/all_gather | solution.py:95
  92.4 210.1 %reduce-scatter.2.cloned.1.call-start = ((), (), s32[]{:S(2)}) async-start(), calls=%async_computation.5 | async-start | bytes 15728640 | tf_op jit(solution)/shard_map/reduce_scatter | solution.py:101
  205.5 1.2 copy-start.4
  206.7 1.2 copy-start.5
  302.5 91.7 %all-to-all-start.2 = ((bf16[8,48,4096]{2,1,0:T(8,128)(2,1)}), bf16[8,48,4096]{2,1,0:T(8,128)(2,1)}, u32[]{:S(2)}, u32[]{:S(2)}) async-start(bf16[8,48,4096]{2,1,0:T(8,128)(2,1)} %bitcast.55), calls=%async_computation.3 | async-start | bytes 6291456 | tf_op jit(solution)/shard_map/all_to_all | solution.py:108
  309.9 68.7 %collective-permute-start = (bf16[15,1024]{1,0:T(8,128)(2,1)S(1)}, bf16[15,1024]{1,0:T(8,128)(2,1)S(1)}, u32[]{:S(2)}, u32[]{:S(2)}) collective-permute-start(bf16[15,1024]{1,0:T(8,128)(2,1)S(1)} %slice.47), channel_id=1, source_target_pairs={{0,4},{4,8},{8,12},{12,16},{16,20},{20,24},{24,28},{1,5},{5,9},{9,... | collective-permute-start | bytes 92168 | tf_op jit(solution)/shard_map/ppermute | solution.py:18
  383.2 1.9 copy-start.2
  389.3 1.6 copy-start.3
  389.3 2.2 copy-start.6
  389.3 2.2 copy-start.7
  398.6 8.3 %copy-start.1 = (bf16[1,256,4096]{2,1,0:T(8,128)(2,1)S(1)}, bf16[1,256,4096]{2,1,0:T(8,128)(2,1)}, u32[]{:S(2)}) copy-start(bf16[1,256,4096]{2,1,0:T(8,128)(2,1)} %param.21) | copy-start | bytes 6291460
Sparse Core Ops, SparseCore 0:
  92.5 83.5 all-gather.1
  205.6 96.7 reduce-scatter.1
where the time goes:
time: 414 us
  waiting for transfers between devices  227 us (55%)
  blocking collectives  90.2 us (22%)
  matrix products  31.9 us (8%)
  local copies, waits for them, and re-layouts  24.3 us (6%)
  other arithmetic  17.4 us (4%)
  between operations  14.3 us (3%)
  starting transfers between devices  9.05 us (2%)
    all_gather x1, waiting for transfers between devices, shards(): piece = lax.all_gather(arrived.reshape(-1, width), 'tp', axis=0, tiled=True)  83.5 us
    reduce_scatter x1, waiting for transfers between devices, shards(): lax.psum_scatter(jnp.dot(hidden, down_local, preferred_element_type=jnp.f...  77.7 us
    all_to_all x1, blocking collectives, shards(): lax.all_to_all(outgoing, 'ep', split_axis=0, concat_axis=0, tiled=True)  74.2 us
    ppermute x1, waiting for transfers between devices, from_behind(): return lax.ppermute(x, axis, pairs)  65.4 us
    dot_general x1, matrix products, shards(): jnp.dot(hidden, down_local, preferred_element_type=jnp.float32)  19.5 us
    all_to_all x1, blocking collectives, shards(): lax.all_to_all(normed, 'tp', split_axis=1, concat_axis=0, tiled=True)  16.1 us
    gather x2, local copies, waits for them, and re-layouts, shards(): flat_rows[slot_index[:, choice_slot]].astype(jnp.float32)  10.1 us
    dot_general x1, matrix products, shards(): jnp.dot(piece, gate_local, preferred_element_type=jnp.float32)  9.87 us
  transfers between devices with their start and end apart: 4, of which 3 were waited for; matrix products, arithmetic and copies ran while one was open for 4% of the time, Pallas kernels for 0%

commit v1 on v0

v1 whole, which is shorter than its diff:
```python
import jax
import jax.numpy as jnp
from jax import lax
from jax.sharding import PartitionSpec as P

WMAX = 16
CHUNKS = 3

epsilon = 1e-06
clamp_limit = 7.0
sigmoid_slope = 1.702


def from_behind(x, axis, by):
    count = lax.axis_size(axis)
    pairs = [(i, i + by) for i in range(count) if 0 <= i + by < count]
    return lax.ppermute(x, axis, pairs)


def rms_norm(values, gain):
    widened = values.astype(jnp.float32)
    scaled = widened * lax.rsqrt(jnp.mean(widened * widened, axis=-1, keepdims=True) + epsilon)
    return (scaled * gain).astype(jnp.bfloat16)


def clamped_unit(gate_part, up_part):
    gate_part = jnp.minimum(gate_part, clamp_limit)
    up_part = jnp.clip(up_part, -clamp_limit, clamp_limit)
    return ((up_part + 1.0) * gate_part * jax.nn.sigmoid(sigmoid_slope * gate_part)).astype(
        jnp.bfloat16
    )


def slot_ids(block_routes, experts, capacity):
    onehot = (
        block_routes[:, :, None] == jnp.arange(experts, dtype=jnp.int32)[None, None, :]
    ).astype(jnp.float32)
    per_token = jnp.sum(onehot, axis=1)
    count = block_routes.shape[0]
    before = (
        jnp.arange(count, dtype=jnp.int32)[:, None] > jnp.arange(count, dtype=jnp.int32)[None, :]
    ).astype(jnp.bfloat16)
    earlier = jnp.dot(before, per_token.astype(jnp.bfloat16), preferred_element_type=jnp.float32)
    rank = jnp.sum(onehot * earlier[:, None, :], axis=2).astype(jnp.int32)
    return block_routes, rank


def mixer(mixer_in, mixer_gain, group_weight, group_scale):
    normed = rms_norm(mixer_in, mixer_gain)
    shard_rows = lax.all_to_all(normed, "tp", split_axis=1, concat_axis=0, tiled=True)
    length = shard_rows.shape[0]
    before = from_behind(shard_rows[length - WMAX :], "ep", 1)
    total = jnp.concatenate([before, shard_rows], axis=0).astype(jnp.float32)
    values = total[WMAX:]
    tp_index = lax.axis_index("tp")
    window = 2 << tp_index
    position = lax.axis_index("ep") * length + jnp.arange(length, dtype=jnp.int32)
    picked = jnp.zeros_like(values)
    reach = 1
    for level in range(lax.axis_size("tp")):
        total = total[reach:] + total[:-reach]
        reach = 2 * reach
        picked = jnp.where(tp_index == level, total[total.shape[0] - length :], picked)
    counts = jnp.minimum(position + 1, window).astype(jnp.float32)[:, None]
    pooled = (picked / counts - values).astype(jnp.bfloat16)
    return (
        jnp.dot(pooled, group_weight[0], preferred_element_type=jnp.float32) * group_scale[0]
    ).astype(jnp.bfloat16)


def shards(
    mixer_in,
    mixer_gain,
    group_weight,
    group_scale,
    expert_in,
    expert_gain,
    routes,
    route_weight,
    gate_weight,
    up_weight,
    down_weight,
):
    mixed = mixer(mixer_in, mixer_gain, group_weight, group_scale)
    expert_norm = rms_norm(expert_in, expert_gain)
    tok_count, width = expert_in.shape
    top = routes.shape[1]
    experts = lax.axis_size("ep")
    capacity = max(2, 3 * tok_count * top // (2 * experts))
    chunks = CHUNKS if capacity % CHUNKS == 0 else 1
    part = capacity // chunks
    tp_index = lax.axis_index("tp")
    own_routes = lax.dynamic_slice_in_dim(routes, tp_index * tok_count, tok_count, 0)
    own_weight = lax.dynamic_slice_in_dim(route_weight, tp_index * tok_count, tok_count, 0)
    gate_local = gate_weight[0]
    up_local = up_weight[0]
    down_full = lax.all_gather(down_weight[0], "tp", axis=0, tiled=True)
    expert_of, rank = slot_ids(own_routes, experts, capacity)
    expert_sum = jnp.zeros((tok_count, width), jnp.float32)
    pieces = []
    picks = []
    for chunk in range(chunks):
        inside = (rank >= chunk * part) & (rank < (chunk + 1) * part)
        slot = jnp.where(inside, expert_of * part + rank - chunk * part, -1)
        match = slot[:, :, None] == jnp.arange(experts * part, dtype=jnp.int32)[None, None, :]
        picks.append(match)
        pick = jnp.any(match, axis=1).astype(jnp.bfloat16)
        outgoing = lax.dot_general(
            pick, expert_norm, (((0,), (0,)), ((), ())), preferred_element_type=jnp.float32
        ).astype(jnp.bfloat16)
        arrived = lax.all_to_all(outgoing, "ep", split_axis=0, concat_axis=0, tiled=True)
        pieces.append(lax.all_gather(arrived, "tp", axis=0, tiled=True))
    for chunk in range(chunks):
        piece = pieces[chunk]
        hidden = clamped_unit(
            jnp.dot(piece, gate_local, preferred_element_type=jnp.float32),
            jnp.dot(piece, up_local, preferred_element_type=jnp.float32),
        )
        hidden = lax.all_to_all(hidden, "tp", split_axis=0, concat_axis=1, tiled=True)
        result = jnp.dot(hidden, down_full, preferred_element_type=jnp.float32).astype(jnp.bfloat16)
        returned = lax.all_to_all(result, "ep", split_axis=0, concat_axis=0, tiled=True)
        weights = jnp.sum(jnp.where(picks[chunk], own_weight[:, :, None], 0.0), axis=1)
        high = weights.astype(jnp.bfloat16)
        low = (weights - high.astype(jnp.float32)).astype(jnp.bfloat16)
        expert_sum = (
            expert_sum
            + jnp.dot(high, returned, preferred_element_type=jnp.float32)
            + jnp.dot(low, returned, preferred_element_type=jnp.float32)
        )
    return (mixed, expert_sum.astype(jnp.bfloat16))


def solution(mesh):
    in_specs = (
        P(("ep", "tp"), None),
        P(),
        P("tp", None, None),
        P("tp", None),
        P(("ep", "tp"), None),
        P(),
        P("ep", None),
        P("ep", None),
        P("ep", None, "tp"),
        P("ep", None, "tp"),
        P("ep", "tp", None),
    )
    out_specs = (P("ep", "tp"), P(("ep", "tp"), None))
    return jax.shard_map(shards, mesh=mesh, in_specs=in_specs, out_specs=out_specs, check_vma=False)
```

time: 414 us -> 338 us (0.82)
  the two profiles are of different devices: /device:TPU:17 before, /device:TPU:0 now
where the time goes in v1:
time: 338 us; the launch traced here: 337 us
  waiting for transfers between devices  101 us (30%)
  blocking collectives  90.9 us (27%)
  matrix products  61.2 us (18%)
  starting transfers between devices  40.5 us (12%)
  local copies, waits for them, and re-layouts  17.7 us (5%)
  between operations  14.1 us (4%)
  other arithmetic  11.8 us (3%)
    all_to_all x3, blocking collectives, shards(): lax.all_to_all(outgoing, 'ep', split_axis=0, concat_axis=0, tiled=True)  90.9 us
    all_gather x1, waiting for transfers between devices, shards(): down_full = lax.all_gather(down_weight[0], 'tp', axis=0, tiled=True)  42.6 us
    all_to_all x3, waiting for transfers between devices, shards(): lax.all_to_all(result, 'ep', split_axis=0, concat_axis=0, tiled=True)  33.2 us
    all_to_all x3, starting transfers between devices, shards(): lax.all_to_all(result, 'ep', split_axis=0, concat_axis=0, tiled=True)  21.9 us
    all_gather x3, waiting for transfers between devices, shards(): pieces.append(lax.all_gather(arrived, 'tp', axis=0, tiled=True))  20.7 us
    dot_general x3, matrix products, shards(): jnp.dot(piece, gate_local, preferred_element_type=jnp.float32)  14.1 us
    dot_general x3, matrix products, shards(): jnp.dot(hidden, down_full, preferred_element_type=jnp.float32)  13.7 us
    dot_general x3, matrix products, shards(): jnp.dot(piece, up_local, preferred_element_type=jnp.float32)  12.4 us
  transfers between devices with their start and end apart: 12, of which 7 were waited for; matrix products, arithmetic and copies ran while one was open for 22% of the time, Pallas kernels for 0%

profile of v1, /device:TPU:0, one launch (start us, length us, event | category | flops | bytes accessed | tf_op | source)
XLA Modules:
  0.0 337.2 jit_solution(14620336182845692313)
XLA Ops:
  9.0 1.5 fusion.19
  10.6 1.8 convolution_convert_fusion.2
  12.3 33.1 %all_to_all.148 = bf16[8,16,4096]{2,1,0:T(8,128)(2,1)} all-to-all(bf16[8,16,4096]{2,1,0:T(8,128)(2,1)S(1)} %bitcast.123), channel_id=1, replica_groups=mesh['ep'=8,'tp'=4] {'ep'}, dimensions={0} | all-to-all | bytes 2097152 | tf_op jit(solution)/shard_map/all_to_all | solution.py:111
  46.2 29.0 %all_to_all.149 = bf16[8,16,4096]{2,1,0:T(8,128)(2,1)} all-to-all(bf16[8,16,4096]{2,1,0:T(8,128)(2,1)S(1)} %bitcast.124), channel_id=1, replica_groups=mesh['ep'=8,'tp'=4] {'ep'}, dimensions={0} | all-to-all | bytes 2097152 | tf_op jit(solution)/shard_map/all_to_all | solution.py:111
  75.8 28.8 %all_to_all.150 = bf16[8,16,4096]{2,1,0:T(8,128)(2,1)} all-to-all(bf16[8,16,4096]{2,1,0:T(8,128)(2,1)S(1)} %bitcast.122), channel_id=1, replica_groups=mesh['ep'=8,'tp'=4] {'ep'}, dimensions={0} | all-to-all | bytes 2097152 | tf_op jit(solution)/shard_map/all_to_all | solution.py:111
  105.3 1.6 copy.39
  107.4 1.5 fusion.18
  108.9 3.5 %all-to-all-start = ((bf16[128,4,1024]{0,2,1:T(8,128)(2,1)}), bf16[128,4,1024]{0,2,1:T(8,128)(2,1)S(1)}, u32[]{:S(2)}, u32[]{:S(2)}) async-start(bf16[128,4,1024]{0,2,1:T(8,128)(2,1)} %bitcast.121), calls=%async_computation | async-start | bytes 2097152 | tf_op jit(solution)/shard_map/all_to_all | solution.py:50
  112.5 4.3 %fusion.43 = f32[512,256]{1,0:T(8,128)S(1)} fusion(bf16[512,4096]{1,0:T(8,128)(2,1)} %all-gather.6.cloned.1.call-done, bf16[1,4096,256]{2,1,0:T(8,128)(2,1)} %param.19), kind=kOutput, calls=%fused_computation.54 | convolution fusion | flops 1073872896 | bytes 6815744 | tf_op jit(solution)/shard_map/dot_general | solution.py:116
  117.3 1.3 fusion.88
  118.6 4.9 %fusion.46 = f32[512,256]{1,0:T(8,128)} fusion(bf16[512,4096]{1,0:T(8,128)(2,1)} %all-gather.8.cloned.1.call-done, bf16[1,4096,256]{2,1,0:T(8,128)(2,1)} %param.19), kind=kOutput, calls=%fused_computation.55 | convolution fusion | flops 1073872896 | bytes 6815744 | tf_op jit(solution)/shard_map/dot_general | solution.py:116
  123.5 0.8 copy.41
  124.3 5.6 %fusion.91 = bf16[512,256]{1,0:T(8,128)(2,1)} fusion(f32[512,256]{1,0:T(8,128)} %fusion.46, bf16[512,4096]{1,0:T(8,128)(2,1)} %all-gather.8.cloned.1.call-done, bf16[1,4096,256]{2,1,0:T(8,128)(2,1)} %param.20), kind=kOutput, calls=%fused_computation.70 | convolution fusion | flops 1074921472 | bytes 7077888 | tf_op jit(solution)/shard_map/dot_general | solution.py:117
  129.9 3.4 %all-to-all-start.2 = ((bf16[4,128,256]{1,2,0:T(8,128)(2,1)}), bf16[4,128,256]{1,2,0:T(8,128)(2,1)S(1)}, u32[]{:S(2)}, u32[]{:S(2)}) async-start(bf16[4,128,256]{1,2,0:T(8,128)(2,1)} %copy.41), calls=%async_computation.2 | async-start | bytes 524288 | tf_op jit(solution)/shard_map/all_to_all | solution.py:119
  133.3 20.7 %all-gather.10.cloned.1.call-done = bf16[512,4096]{1,0:T(8,128)(2,1)} async-done(((bf16[128,4096]{1,0:T(8,128)(2,1)}), bf16[512,4096]{1,0:T(8,128)(2,1)}) %all-gather.10.cloned.1.call-update) | async-done | bytes 4194320 | tf_op jit(solution)/shard_map/all_gather | solution.py:112
  154.0 4.9 %fusion.49 = f32[512,256]{1,0:T(8,128)} fusion(bf16[512,4096]{1,0:T(8,128)(2,1)} %all-gather.10.cloned.1.call-done, bf16[1,4096,256]{2,1,0:T(8,128)(2,1)} %param.19), kind=kOutput, calls=%fused_computation.56 | convolution fusion | flops 1073872896 | bytes 6815744 | tf_op jit(solution)/shard_map/dot_general | solution.py:116
  158.9 1.8 copy.42
  160.7 3.4 %all-to-all-start.5 = ((bf16[4,128,256]{1,2,0:T(8,128)(2,1)}), bf16[4,128,256]{1,2,0:T(8,128)(2,1)S(1)}, u32[]{:S(2)}, u32[]{:S(2)}) async-start(bf16[4,128,256]{1,2,0:T(8,128)(2,1)} %copy.42), calls=%async_computation.5 | async-start | bytes 524288 | tf_op jit(solution)/shard_map/all_to_all | solution.py:119
  164.2 5.5 %fusion.94 = bf16[512,256]{1,0:T(8,128)(2,1)S(1)} fusion(f32[512,256]{1,0:T(8,128)} %fusion.49, bf16[512,4096]{1,0:T(8,128)(2,1)} %all-gather.10.cloned.1.call-done, bf16[1,4096,256]{2,1,0:T(8,128)(2,1)} %param.20), kind=kOutput, calls=%fused_computation.71 | convolution fusion | flops 1074921472 | bytes 7077888 | tf_op jit(solution)/shard_map/dot_general | solution.py:117
  169.7 0.8 copy.43
  170.6 2.6 all-to-all-done.5
  173.1 3.6 %all-to-all-start.8 = ((bf16[4,128,256]{1,2,0:T(8,128)(2,1)}), bf16[4,128,256]{1,2,0:T(8,128)(2,1)S(1)}, u32[]{:S(2)}, u32[]{:S(2)}) async-start(bf16[4,128,256]{1,2,0:T(8,128)(2,1)} %copy.43), calls=%async_computation.8 | async-start | bytes 524288 | tf_op jit(solution)/shard_map/all_to_all | solution.py:119
  176.7 42.6 %all-gather.12.cloned.1.call-done = bf16[1,1024,4096]{2,1,0:T(8,128)(2,1)} async-done(((bf16[1,256,4096]{2,1,0:T(8,128)(2,1)}), bf16[1,1024,4096]{2,1,0:T(8,128)(2,1)}) %all-gather.12.cloned.1.call-update) | async-done | bytes 8388624 | tf_op jit(solution)/shard_map/all_gather | solution.py:97
  219.3 5.8 %fusion.7 = bf16[128,4096]{1,0:T(8,128)(2,1)} fusion(bf16[128,1024]{0,1:T(8,128)(2,1)} %bitcast.134, bf16[1,1024,4096]{2,1,0:T(8,128)(2,1)} %all-gather.12.cloned.1.call-done), kind=kOutput, calls=%fused_computation.12 | convolution fusion | flops 1074266112 | bytes 9699328 | tf_op jit(solution)/shard_map/dot_general | solution.py:120
  225.1 5.5 %all-to-all-start.3 = ((bf16[8,16,4096]{2,1,0:T(8,128)(2,1)}), bf16[8,16,4096]{2,1,0:T(8,128)(2,1)S(1)}, u32[]{:S(2)}, u32[]{:S(2)}) async-start(bf16[8,16,4096]{2,1,0:T(8,128)(2,1)} %bitcast.129), calls=%async_computation.3 | async-start | bytes 2097152 | tf_op jit(solution)/shard_map/all_to_all | solution.py:121
  231.3 0.8 select_reduce_fusion
  232.1 2.3 copy.40
  234.4 1.4 slice.56
  235.8 4.5 %collective-permute-start = (bf16[16,1024]{1,0:T(8,128)(2,1)}, bf16[16,1024]{1,0:T(8,128)(2,1)}, u32[]{:S(2)}, u32[]{:S(2)}) collective-permute-start(bf16[16,1024]{1,0:T(8,128)(2,1)} %slice.56), channel_id=1, source_target_pairs={{0,4},{4,8},{8,12},{12,16},{16,20},{20,24},{24,28},{1,5},{5,9},{9,... | collective-permute-start | bytes 98312 | tf_op jit(solution)/shard_map/ppermute | solution.py:17
  240.3 1.3 collective-permute-done
  241.6 2.9 maximum_convert_fusion
  244.5 5.6 %fusion.10 = bf16[128,4096]{1,0:T(8,128)(2,1)} fusion(bf16[128,1024]{0,1:T(8,128)(2,1)S(1)} %bitcast.133, bf16[1,1024,4096]{2,1,0:T(8,128)(2,1)} %all-gather.12.cloned.1.call-done), kind=kOutput, calls=%fused_computation.13 | convolution fusion | flops 1074266112 | bytes 9699328 | tf_op jit(solution)/shard_map/dot_general | solution.py:120
  250.2 6.6 %all-to-all-done.3 = bf16[8,16,4096]{2,1,0:T(8,128)(2,1)S(1)} async-done(((bf16[8,16,4096]{2,1,0:T(8,128)(2,1)}), bf16[8,16,4096]{2,1,0:T(8,128)(2,1)S(1)}, u32[]{:S(2)}, u32[]{:S(2)}) %all-to-all-start.3) | async-done | bytes 1048608 | tf_op jit(solution)/shard_map/all_to_all | solution.py:121
  256.8 12.1 %all-to-all-start.6 = ((bf16[8,16,4096]{2,1,0:T(8,128)(2,1)}), bf16[8,16,4096]{2,1,0:T(8,128)(2,1)}, u32[]{:S(2)}, u32[]{:S(2)}) async-start(bf16[8,16,4096]{2,1,0:T(8,128)(2,1)} %bitcast.131), calls=%async_computation.6 | async-start | bytes 2097152 | tf_op jit(solution)/shard_map/all_to_all | solution.py:121
  268.9 2.8 slice_add_fusion.2
  272.0 1.1 copy-done.1
  273.5 0.9 copy-done.2
  274.4 2.6 fusion.114
  277.6 1.4 slice-done.1
  279.0 2.3 fusion.13
  281.2 14.5 %all-to-all-done.6 = bf16[8,16,4096]{2,1,0:T(8,128)(2,1)} async-done(((bf16[8,16,4096]{2,1,0:T(8,128)(2,1)}), bf16[8,16,4096]{2,1,0:T(8,128)(2,1)}, u32[]{:S(2)}, u32[]{:S(2)}) %all-to-all-start.6) | async-done | bytes 1048608 | tf_op jit(solution)/shard_map/all_to_all | solution.py:121
  295.8 4.2 %all-to-all-start.9 = ((bf16[8,16,4096]{2,1,0:T(8,128)(2,1)}), bf16[8,16,4096]{2,1,0:T(8,128)(2,1)}, u32[]{:S(2)}, u32[]{:S(2)}) async-start(bf16[8,16,4096]{2,1,0:T(8,128)(2,1)} %bitcast.130), calls=%async_computation.9 | async-start | bytes 2097152 | tf_op jit(solution)/shard_map/all_to_all | solution.py:121
  300.0 7.7 %multiply_convert_fusion = bf16[512,1024]{1,0:T(8,128)(2,1)} fusion(bf16[1,1024,1024]{2,1,0:T(8,128)(2,1)S(1)} %copy-done, f32[1024]{0:T(1024)S(1)} %bitcast.138, f32[528,1024]{1,0:T(8,128)} %maximum_convert_fusion, f32[527,1024]{1,0:T(8,128)} %copy-done.1, f32[525,1024]{1,0:T(8,128)} %copy-done.2, f32[521,1024]{1,0:T(8,128)} %copy-done.3, ...), kind=kOutput, calls=%fused_computation.53 | convolution fusion | flops 1078984704 | bytes 15734788 | tf_op jit(solution)/shard_map/dot_general | solution.py:67
  309.0 1.6 convolution_add_fusion.3
  310.6 3.0 convolution_add_fusion.2
  313.6 12.1 %all-to-all-done.9 = bf16[8,16,4096]{2,1,0:T(8,128)(2,1)} async-done(((bf16[8,16,4096]{2,1,0:T(8,128)(2,1)}), bf16[8,16,4096]{2,1,0:T(8,128)(2,1)}, u32[]{:S(2)}, u32[]{:S(2)}) %all-to-all-start.9) | async-done | bytes 1048608 | tf_op jit(solution)/shard_map/all_to_all | solution.py:121
  325.7 2.3 convolution_add_fusion.1
  328.0 2.6 fusion.6
  (63 shorter events, 8.1 us)
Async XLA Ops:
  7.2 292.9 %copy-start = (bf16[1,1024,1024]{2,1,0:T(8,128)(2,1)S(1)}, bf16[1,1024,1024]{2,1,0:T(8,128)(2,1)}, u32[]{:S(2)}) copy-start(bf16[1,1024,1024]{2,1,0:T(8,128)(2,1)} %param.13) | copy-start | bytes 6291460
  7.2 105.3 %all-gather.6.cloned.1.call-start = ((), (), s32[]{:S(2)}) async-start(), calls=%async_computation.10 | async-start | bytes 5242880 | tf_op jit(solution)/shard_map/all_gather | solution.py:112
  12.3 33.4 %copy-start.4 = (bf16[128,4096]{1,0:T(8,128)(2,1)S(1)}, bf16[128,4096]{1,0:T(8,128)(2,1)}, u32[]{:S(2)}) copy-start(bf16[128,4096]{1,0:T(8,128)(2,1)} %param.15) | copy-start | bytes 3145732
  12.3 33.4 %copy-start.10 = (f32[4096]{0:T(1024)S(1)}, f32[4096]{0:T(1024)}, u32[]{:S(2)}) copy-start(f32[4096]{0:T(1024)} %param.16) | copy-start | bytes 49156
  45.5 73.1 %all-gather.8.cloned.1.call-start = ((), (), s32[]{:S(2)}) async-start(), calls=%async_computation.11 | async-start | bytes 5242880 | tf_op jit(solution)/shard_map/all_gather | solution.py:112
  75.2 78.8 %all-gather.10.cloned.1.call-start = ((), (), s32[]{:S(2)}) async-start(), calls=%async_computation.12 | async-start | bytes 5242880 | tf_op jit(solution)/shard_map/all_gather | solution.py:112
  104.7 114.7 %all-gather.12.cloned.1.call-start = ((), (), s32[]{:S(2)}) async-start(), calls=%async_computation.13 | async-start | bytes 10485760 | tf_op jit(solution)/shard_map/all_gather | solution.py:97
  105.2 2.2 copy-start.11
  108.9 20.9 %all-to-all-start = ((bf16[128,4,1024]{0,2,1:T(8,128)(2,1)}), bf16[128,4,1024]{0,2,1:T(8,128)(2,1)S(1)}, u32[]{:S(2)}, u32[]{:S(2)}) async-start(bf16[128,4,1024]{0,2,1:T(8,128)(2,1)} %bitcast.121), calls=%async_computation | async-start | bytes 2097152 | tf_op jit(solution)/shard_map/all_to_all | solution.py:50
  112.5 4.3 %copy-start.12 = (bf16[512,4096]{1,0:T(8,128)(2,1)S(1)}, bf16[512,4096]{1,0:T(8,128)(2,1)}, u32[]{:S(2)}) copy-start(bf16[512,4096]{1,0:T(8,128)(2,1)} %all-gather.6.cloned.1.call-done) | copy-start | bytes 12582916
  112.5 4.8 %copy-start.13 = (bf16[1,4096,256]{2,1,0:T(8,128)(2,1)S(1)}, bf16[1,4096,256]{2,1,0:T(8,128)(2,1)}, u32[]{:S(2)}) copy-start(bf16[1,4096,256]{2,1,0:T(8,128)(2,1)} %param.20) | copy-start | bytes 6291460
  129.9 29.0 %copy-start.5 = (bf16[128,4,1024]{0,2,1:T(8,128)(2,1)}, bf16[128,4,1024]{0,2,1:T(8,128)(2,1)S(1)}, u32[]{:S(2)}) copy-start(bf16[128,4,1024]{0,2,1:T(8,128)(2,1)S(1)} %all-to-all-done) | copy-start | bytes 3145732
  129.9 30.8 %all-to-all-start.2 = ((bf16[4,128,256]{1,2,0:T(8,128)(2,1)}), bf16[4,128,256]{1,2,0:T(8,128)(2,1)S(1)}, u32[]{:S(2)}, u32[]{:S(2)}) async-start(bf16[4,128,256]{1,2,0:T(8,128)(2,1)} %copy.41), calls=%async_computation.2 | async-start | bytes 524288 | tf_op jit(solution)/shard_map/all_to_all | solution.py:119
  160.7 9.0 %copy-start.8 = (bf16[4,128,256]{1,2,0:T(8,128)(2,1)}, bf16[4,128,256]{1,2,0:T(8,128)(2,1)S(1)}, u32[]{:S(2)}) copy-start(bf16[4,128,256]{1,2,0:T(8,128)(2,1)S(1)} %all-to-all-done.2) | copy-start | bytes 786436
  160.7 12.4 %all-to-all-start.5 = ((bf16[4,128,256]{1,2,0:T(8,128)(2,1)}), bf16[4,128,256]{1,2,0:T(8,128)(2,1)S(1)}, u32[]{:S(2)}, u32[]{:S(2)}) async-start(bf16[4,128,256]{1,2,0:T(8,128)(2,1)} %copy.42), calls=%async_computation.5 | async-start | bytes 524288 | tf_op jit(solution)/shard_map/all_to_all | solution.py:119
  173.1 52.0 %copy-start.6 = (bf16[4,128,256]{1,2,0:T(8,128)(2,1)}, bf16[4,128,256]{1,2,0:T(8,128)(2,1)S(1)}, u32[]{:S(2)}) copy-start(bf16[4,128,256]{1,2,0:T(8,128)(2,1)S(1)} %all-to-all-done.5) | copy-start | bytes 786436
  173.1 52.0 %all-to-all-start.8 = ((bf16[4,128,256]{1,2,0:T(8,128)(2,1)}), bf16[4,128,256]{1,2,0:T(8,128)(2,1)S(1)}, u32[]{:S(2)}, u32[]{:S(2)}) async-start(bf16[4,128,256]{1,2,0:T(8,128)(2,1)} %copy.43), calls=%async_computation.8 | async-start | bytes 524288 | tf_op jit(solution)/shard_map/all_to_all | solution.py:119
  225.1 31.7 %all-to-all-start.3 = ((bf16[8,16,4096]{2,1,0:T(8,128)(2,1)}), bf16[8,16,4096]{2,1,0:T(8,128)(2,1)S(1)}, u32[]{:S(2)}, u32[]{:S(2)}) async-start(bf16[8,16,4096]{2,1,0:T(8,128)(2,1)} %bitcast.129), calls=%async_computation.3 | async-start | bytes 2097152 | tf_op jit(solution)/shard_map/all_to_all | solution.py:121
  235.8 5.9 %collective-permute-start = (bf16[16,1024]{1,0:T(8,128)(2,1)}, bf16[16,1024]{1,0:T(8,128)(2,1)}, u32[]{:S(2)}, u32[]{:S(2)}) collective-permute-start(bf16[16,1024]{1,0:T(8,128)(2,1)} %slice.56), channel_id=1, source_target_pairs={{0,4},{4,8},{8,12},{12,16},{16,20},{20,24},{24,28},{1,5},{5,9},{9,... | collective-permute-start | bytes 98312 | tf_op jit(solution)/shard_map/ppermute | solution.py:17
  240.3 4.2 %copy-start.7 = (bf16[4,128,256]{1,2,0:T(8,128)(2,1)S(1)}, bf16[4,128,256]{1,2,0:T(8,128)(2,1)}, u32[]{:S(2)}) copy-start(bf16[4,128,256]{1,2,0:T(8,128)(2,1)} %copy-done.6) | copy-start | bytes 786436
  256.8 39.0 %all-to-all-start.6 = ((bf16[8,16,4096]{2,1,0:T(8,128)(2,1)}), bf16[8,16,4096]{2,1,0:T(8,128)(2,1)}, u32[]{:S(2)}, u32[]{:S(2)}) async-start(bf16[8,16,4096]{2,1,0:T(8,128)(2,1)} %bitcast.131), calls=%async_computation.6 | async-start | bytes 2097152 | tf_op jit(solution)/shard_map/all_to_all | solution.py:121
  271.7 1.4 copy-start.1
  271.7 5.9 %slice-start = ((s8[8388608]{0:T(1024)(128)(4,1)}), s8[4194304]{0:T(1024)(128)(4,1)S(1)}, s32[]{:S(2)}) async-start(s8[8388608]{0:T(1024)(128)(4,1)} %bitcast.115), calls=%async_computation.14 | async-start | bytes 8388608
  273.0 1.3 copy-start.2
  273.1 5.9 %slice-start.1 = ((s8[8388608]{0:T(1024)(128)(4,1)}), s8[4194304]{0:T(1024)(128)(4,1)S(1)}, s32[]{:S(2)}) async-start(s8[8388608]{0:T(1024)(128)(4,1)} %bitcast.115), calls=%async_computation.15 | async-start | bytes 8388608
  274.4 3.2 copy-start.3
  281.2 18.8 %copy-start.14 = (f32[1,1024]{1,0:T(1,128)S(1)}, f32[1,1024]{1,0:T(1,128)}, u32[]{:S(2)}) copy-start(f32[1,1024]{1,0:T(1,128)} %param.14) | copy-start | bytes 12292
  295.8 29.9 %all-to-all-start.9 = ((bf16[8,16,4096]{2,1,0:T(8,128)(2,1)}), bf16[8,16,4096]{2,1,0:T(8,128)(2,1)}, u32[]{:S(2)}, u32[]{:S(2)}) async-start(bf16[8,16,4096]{2,1,0:T(8,128)(2,1)} %bitcast.130), calls=%async_computation.9 | async-start | bytes 2097152 | tf_op jit(solution)/shard_map/all_to_all | solution.py:121
  308.1 0.8 copy-start.9
Sparse Core Ops, SparseCore 0:
  45.6 33.4 all-gather.5
  80.7 34.4 all-gather.7
  116.7 37.2 all-gather.9
  155.4 63.8 all-gather.11

commit v2 on v1

--- a/solution.py
+++ b/solution.py
@@ -45,11 +45,15 @@
     return block_routes, rank
 
 
-def mixer(mixer_in, mixer_gain, group_weight, group_scale):
+def mixer_rows(mixer_in, mixer_gain):
     normed = rms_norm(mixer_in, mixer_gain)
     shard_rows = lax.all_to_all(normed, "tp", split_axis=1, concat_axis=0, tiled=True)
     length = shard_rows.shape[0]
-    before = from_behind(shard_rows[length - WMAX :], "ep", 1)
+    return shard_rows, from_behind(shard_rows[length - WMAX :], "ep", 1)
+
+
+def mixer(shard_rows, before, group_weight, group_scale):
+    length = shard_rows.shape[0]
     total = jnp.concatenate([before, shard_rows], axis=0).astype(jnp.float32)
     values = total[WMAX:]
     tp_index = lax.axis_index("tp")
@@ -81,7 +85,9 @@
     up_weight,
     down_weight,
 ):
-    mixed = mixer(mixer_in, mixer_gain, group_weight, group_scale)
+    shard_rows, before = mixer_rows(mixer_in, mixer_gain)
+    expert_in, shard_rows, before = lax.optimization_barrier((expert_in, shard_rows, before))
+    mixed = mixer(shard_rows, before, group_weight, group_scale)
     expert_norm = rms_norm(expert_in, expert_gain)
     tok_count, width = expert_in.shape
     top = routes.shape[1]
@@ -108,10 +114,16 @@
         outgoing = lax.dot_general(
             pick, expert_norm, (((0,), (0,)), ((), ())), preferred_element_type=jnp.float32
         ).astype(jnp.bfloat16)
+        if chunk > 0:
+            outgoing, arrived = lax.optimization_barrier((outgoing, arrived))
         arrived = lax.all_to_all(outgoing, "ep", split_axis=0, concat_axis=0, tiled=True)
+        if chunk == 1:
+            arrived, down_full = lax.optimization_barrier((arrived, down_full))
         pieces.append(lax.all_gather(arrived, "tp", axis=0, tiled=True))
     for chunk in range(chunks):
         piece = pieces[chunk]
+        if chunk > 0:
+            piece, result = lax.optimization_barrier((piece, result))
         hidden = clamped_unit(
             jnp.dot(piece, gate_local, preferred_element_type=jnp.float32),
             jnp.dot(piece, up_local, preferred_element_type=jnp.float32),

time: 338 us -> 289 us (0.86)
  waiting for transfers between devices: 101 us -> 64.7 us
  blocking collectives: 90.9 us -> 108 us
  starting transfers between devices: 40.5 us -> 25.8 us
  matrix products: 61.2 us -> 50.7 us
    all_gather x1, waiting for transfers between devices: 42.6 us -> 0.01 us  [shards(): down_full = lax.all_gather(down_weight[0], 'tp', axis=0, tiled=True)]
    all_to_all x1, waiting for transfers between devices: 0.01 us -> 22.9 us  [mixer_rows(): lax.all_to_all(normed, 'tp', split_axis=1, concat_axis=0, tiled=True)]
    all_to_all x0 -> x2, blocking collectives: none -> 20.5 us  [shards(): lax.all_to_all(hidden, 'tp', split_axis=0, concat_axis=1, tiled=True)]
    all_gather x3, waiting for transfers between devices: 20.7 us -> 1.89 us  [shards(): pieces.append(lax.all_gather(arrived, 'tp', axis=0, tiled=True))]
    all_to_all x3, starting transfers between devices: 21.9 us -> 12.5 us  [shards(): lax.all_to_all(result, 'ep', split_axis=0, concat_axis=0, tiled=True)]
    dot_general x3, matrix products: 12.4 us -> 3.77 us  [shards(): jnp.dot(piece, up_local, preferred_element_type=jnp.float32)]
    all_to_all x3 -> x1, starting transfers between devices: 10.4 us -> 3.4 us  [shards(): lax.all_to_all(hidden, 'tp', split_axis=0, concat_axis=1, tiled=True)]
    all_to_all x3, blocking collectives: 90.9 us -> 87.3 us  [shards(): lax.all_to_all(outgoing, 'ep', split_axis=0, concat_axis=0, tiled=True)]
  transfers between devices with their start and end apart: 12 -> 10, of which waited for: 7 -> 7; matrix products, arithmetic and copies ran while one was open for 22% -> 22% of each run, Pallas kernels for 0% -> 0%
where the time goes in v2:
time: 289 us; the launch traced here: 288 us
  blocking collectives  108 us (37%)
  waiting for transfers between devices  64.7 us (22%)
  matrix products  50.7 us (18%)
  starting transfers between devices  25.8 us (9%)
  local copies, waits for them, and re-layouts  15.6 us (5%)
  between operations  14.1 us (5%)
  other arithmetic  9.82 us (3%)
    all_to_all x3, blocking collectives, shards(): lax.all_to_all(outgoing, 'ep', split_axis=0, concat_axis=0, tiled=True)  87.3 us
    all_to_all x3, waiting for transfers between devices, shards(): lax.all_to_all(result, 'ep', split_axis=0, concat_axis=0, tiled=True)  35.2 us
    all_to_all x1, waiting for transfers between devices, mixer_rows(): lax.all_to_all(normed, 'tp', split_axis=1, concat_axis=0, tiled=True)  22.9 us
    all_to_all x2, blocking collectives, shards(): lax.all_to_all(hidden, 'tp', split_axis=0, concat_axis=1, tiled=True)  20.5 us
    dot_general x3, matrix products, shards(): jnp.dot(hidden, down_full, preferred_element_type=jnp.float32)  13.6 us
    dot_general x3, matrix products, shards(): jnp.dot(piece, gate_local, preferred_element_type=jnp.float32)  13.4 us
    all_to_all x3, starting transfers between devices, shards(): lax.all_to_all(result, 'ep', split_axis=0, concat_axis=0, tiled=True)  12.5 us
    unnamed x37, local copies, waits for them, and re-layouts  8.1 us
  transfers between devices with their start and end apart: 10, of which 7 were waited for; matrix products, arithmetic and copies ran while one was open for 22% of the time, Pallas kernels for 0%

profile of v2, /device:TPU:0, one launch (start us, length us, event | category | flops | bytes accessed | tf_op | source)
XLA Modules:
  0.0 288.4 jit_solution(611450616829126164)
XLA Ops:
  7.2 0.7 all-gather.12.cloned.1.call-update
  7.9 1.6 copy.39
  10.1 1.5 fusion.3
  11.6 4.4 %all-to-all-start = ((bf16[128,4,1024]{0,2,1:T(8,128)(2,1)}), bf16[128,4,1024]{0,2,1:T(8,128)(2,1)}, u32[]{:S(2)}, u32[]{:S(2)}) async-start(bf16[128,4,1024]{0,2,1:T(8,128)(2,1)} %bitcast.115), calls=%async_computation | async-start | bytes 2097152 | tf_op jit(solution)/shard_map/all_to_all | solution.py:50
  16.3 22.9 %all-to-all-done = bf16[128,4,1024]{0,2,1:T(8,128)(2,1)} async-done(((bf16[128,4,1024]{0,2,1:T(8,128)(2,1)}), bf16[128,4,1024]{0,2,1:T(8,128)(2,1)}, u32[]{:S(2)}, u32[]{:S(2)}) %all-to-all-start) | async-done | bytes 1048608 | tf_op jit(solution)/shard_map/all_to_all | solution.py:50
  39.2 2.3 copy.40
  41.5 0.8 slice.56
  42.3 5.4 %collective-permute-start = (bf16[16,1024]{1,0:T(8,128)(2,1)S(1)}, bf16[16,1024]{1,0:T(8,128)(2,1)}, u32[]{:S(2)}, u32[]{:S(2)}) collective-permute-start(bf16[16,1024]{1,0:T(8,128)(2,1)S(1)} %slice.56), channel_id=1, source_target_pairs={{0,4},{4,8},{8,12},{12,16},{16,20},{20,24},{24,28},{1,5},{5,9},{9,... | collective-permute-start | bytes 98312 | tf_op jit(solution)/shard_map/ppermute | solution.py:17
  47.8 0.8 collective-permute-done
  49.4 30.4 %all_to_all.148 = bf16[8,16,4096]{2,1,0:T(8,128)(2,1)} all-to-all(bf16[8,16,4096]{2,1,0:T(8,128)(2,1)S(1)} %bitcast.117), channel_id=1, replica_groups=mesh['ep'=8,'tp'=4] {'ep'}, dimensions={0} | all-to-all | bytes 2097152 | tf_op jit(solution)/shard_map/all_to_all | solution.py:119
  80.5 28.0 %all_to_all.149 = bf16[8,16,4096]{2,1,0:T(8,128)(2,1)} all-to-all(bf16[8,16,4096]{2,1,0:T(8,128)(2,1)S(1)} %bitcast.118), channel_id=1, replica_groups=mesh['ep'=8,'tp'=4] {'ep'}, dimensions={0} | all-to-all | bytes 2097152 | tf_op jit(solution)/shard_map/all_to_all | solution.py:119
  109.1 28.9 %all_to_all.150 = bf16[8,16,4096]{2,1,0:T(8,128)(2,1)} all-to-all(bf16[8,16,4096]{2,1,0:T(8,128)(2,1)S(1)} %bitcast.116), channel_id=1, replica_groups=mesh['ep'=8,'tp'=4] {'ep'}, dimensions={0} | all-to-all | bytes 2097152 | tf_op jit(solution)/shard_map/all_to_all | solution.py:119
  138.1 4.3 %fusion.28 = f32[512,256]{1,0:T(8,128)S(1)} fusion(bf16[512,4096]{1,0:T(8,128)(2,1)} %all-gather.6.cloned.1.call-done, bf16[1,4096,256]{2,1,0:T(8,128)(2,1)} %param.19), kind=kOutput, calls=%fused_computation.48 | convolution fusion | flops 1073872896 | bytes 6815744 | tf_op jit(solution)/shard_map/dot_general | solution.py:128
  142.9 1.3 fusion.73
  144.3 8.8 %all_to_all.151 = bf16[4,128,256]{1,2,0:T(8,128)(2,1)S(1)} all-to-all(bf16[4,128,256]{1,2,0:T(8,128)(2,1)S(1)} %copy.41), channel_id=1, replica_groups=mesh['ep'=8,'tp'=4] {'tp'}, dimensions={0} | all-to-all | bytes 524288 | tf_op jit(solution)/shard_map/all_to_all | solution.py:131
  153.2 5.6 %convolution_convert_fusion.3 = bf16[128,4096]{1,0:T(8,128)(2,1)} fusion(bf16[128,1024]{0,1:T(8,128)(2,1)S(1)} %bitcast.127, bf16[1024,4096]{1,0:T(8,128)(2,1)} %bitcast.106), kind=kOutput, calls=%fused_computation.9 | convolution fusion | flops 1074266112 | bytes 9699328 | tf_op jit(solution)/shard_map/dot_general | solution.py:132
  158.8 4.9 %fusion.31 = f32[512,256]{1,0:T(8,128)S(1)} fusion(bf16[512,4096]{1,0:T(8,128)(2,1)} %all-gather.8.cloned.1.call-done, bf16[1,4096,256]{2,1,0:T(8,128)(2,1)} %param.19), kind=kOutput, calls=%fused_computation.49 | convolution fusion | flops 1073872896 | bytes 6815744 | tf_op jit(solution)/shard_map/dot_general | solution.py:128
  164.2 0.7 copy-done.13
  164.9 1.3 fusion.76
  166.4 11.6 %all_to_all.152 = bf16[4,128,256]{1,2,0:T(8,128)(2,1)S(1)} all-to-all(bf16[4,128,256]{1,2,0:T(8,128)(2,1)S(1)} %copy.42), channel_id=1, replica_groups=mesh['ep'=8,'tp'=4] {'tp'}, dimensions={0} | all-to-all | bytes 524288 | tf_op jit(solution)/shard_map/all_to_all | solution.py:131
  178.0 4.0 %all-to-all-start.4 = ((bf16[8,16,4096]{2,1,0:T(8,128)(2,1)}), bf16[8,16,4096]{2,1,0:T(8,128)(2,1)S(1)}, u32[]{:S(2)}, u32[]{:S(2)}) async-start(bf16[8,16,4096]{2,1,0:T(8,128)(2,1)} %bitcast.123), calls=%async_computation.4 | async-start | bytes 2097152 | tf_op jit(solution)/shard_map/all_to_all | solution.py:133
  182.0 0.7 constant_dynamic-slice_fusion
  182.7 0.8 select_reduce_fusion
  183.5 5.7 %convolution_convert_fusion.2 = bf16[128,4096]{1,0:T(8,128)(2,1)} fusion(bf16[128,1024]{0,1:T(8,128)(2,1)S(1)} %bitcast.126, bf16[1024,4096]{1,0:T(8,128)(2,1)} %bitcast.107), kind=kOutput, calls=%fused_computation.8 | convolution fusion | flops 1074266112 | bytes 9699328 | tf_op jit(solution)/shard_map/dot_general | solution.py:132
  189.2 1.9 all-gather.10.cloned.1.call-done
  191.1 4.3 %fusion.34 = f32[512,256]{1,0:T(8,128)S(1)} fusion(bf16[512,4096]{1,0:T(8,128)(2,1)} %all-gather.10.cloned.1.call-done, bf16[1,4096,256]{2,1,0:T(8,128)(2,1)} %param.19), kind=kOutput, calls=%fused_computation.50 | convolution fusion | flops 1073872896 | bytes 6815744 | tf_op jit(solution)/shard_map/dot_general | solution.py:128
  195.8 1.3 fusion.79
  197.1 0.8 copy.43
  197.9 9.8 %all-to-all-done.4 = bf16[8,16,4096]{2,1,0:T(8,128)(2,1)S(1)} async-done(((bf16[8,16,4096]{2,1,0:T(8,128)(2,1)}), bf16[8,16,4096]{2,1,0:T(8,128)(2,1)S(1)}, u32[]{:S(2)}, u32[]{:S(2)}) %all-to-all-start.4) | async-done | bytes 1048608 | tf_op jit(solution)/shard_map/all_to_all | solution.py:133
  207.7 3.4 %all-to-all-start.8 = ((bf16[4,128,256]{1,2,0:T(8,128)(2,1)}), bf16[4,128,256]{1,2,0:T(8,128)(2,1)S(1)}, u32[]{:S(2)}, u32[]{:S(2)}) async-start(bf16[4,128,256]{1,2,0:T(8,128)(2,1)} %copy.43), calls=%async_computation.8 | async-start | bytes 524288 | tf_op jit(solution)/shard_map/all_to_all | solution.py:131
  211.2 2.9 %maximum_convert_fusion = f32[528,1024]{1,0:T(8,128)} fusion(bf16[512,1024]{1,0:T(8,128)(2,1)} %bitcast.114, bf16[16,1024]{1,0:T(8,128)(2,1)} %collective-permute-done), kind=kLoop, calls=%fused_computation.66 | loop fusion | flops 2162688 | bytes 3244032 | tf_op jit(solution)/shard_map/convert_element_type | solution.py:57
  214.1 3.0 %all-to-all-done.8 = bf16[4,128,256]{1,2,0:T(8,128)(2,1)S(1)} async-done(((bf16[4,128,256]{1,2,0:T(8,128)(2,1)}), bf16[4,128,256]{1,2,0:T(8,128)(2,1)S(1)}, u32[]{:S(2)}, u32[]{:S(2)}) %all-to-all-start.8) | async-done | bytes 262176 | tf_op jit(solution)/shard_map/all_to_all | solution.py:131
  217.1 4.2 %all-to-all-start.6 = ((bf16[8,16,4096]{2,1,0:T(8,128)(2,1)}), bf16[8,16,4096]{2,1,0:T(8,128)(2,1)}, u32[]{:S(2)}, u32[]{:S(2)}) async-start(bf16[8,16,4096]{2,1,0:T(8,128)(2,1)} %bitcast.122), calls=%async_computation.6 | async-start | bytes 2097152 | tf_op jit(solution)/shard_map/all_to_all | solution.py:133
  221.4 2.7 slice_add_fusion.2
  224.4 1.1 copy-done.1
  225.9 0.9 copy-done.2
  226.8 2.6 fusion.99
  229.4 0.6 copy-done.3
  230.0 1.4 slice-done.1
  231.4 2.3 convolution_convert_fusion
  233.6 13.5 %all-to-all-done.6 = bf16[8,16,4096]{2,1,0:T(8,128)(2,1)} async-done(((bf16[8,16,4096]{2,1,0:T(8,128)(2,1)}), bf16[8,16,4096]{2,1,0:T(8,128)(2,1)}, u32[]{:S(2)}, u32[]{:S(2)}) %all-to-all-start.6) | async-done | bytes 1048608 | tf_op jit(solution)/shard_map/all_to_all | solution.py:133
  247.1 4.2 %all-to-all-start.9 = ((bf16[8,16,4096]{2,1,0:T(8,128)(2,1)}), bf16[8,16,4096]{2,1,0:T(8,128)(2,1)}, u32[]{:S(2)}, u32[]{:S(2)}) async-start(bf16[8,16,4096]{2,1,0:T(8,128)(2,1)} %bitcast.124), calls=%async_computation.9 | async-start | bytes 2097152 | tf_op jit(solution)/shard_map/all_to_all | solution.py:133
  251.4 7.7 %multiply_convert_fusion = bf16[512,1024]{1,0:T(8,128)(2,1)} fusion(bf16[1,1024,1024]{2,1,0:T(8,128)(2,1)S(1)} %copy-done, f32[1024]{0:T(1024)S(1)} %bitcast.131, f32[528,1024]{1,0:T(8,128)} %maximum_convert_fusion, f32[527,1024]{1,0:T(8,128)} %copy-done.1, f32[525,1024]{1,0:T(8,128)} %copy-done.2, f32[521,1024]{1,0:T(8,128)} %copy-done.3, ...), kind=kOutput, calls=%fused_computation.47 | convolution fusion | flops 1078984704 | bytes 15734788 | tf_op jit(solution)/shard_map/dot_general | solution.py:71
  260.3 1.6 convolution_add_fusion.3
  261.9 3.0 %convolution_add_fusion.2 = f32[128,4096]{1,0:T(8,128)} fusion(f32[128,4096]{1,0:T(8,128)S(1)} %convolution_add_fusion.3, bf16[128,4096]{1,0:T(8,128)(2,1)} %bitcast.21, f32[128,128]{1,0:T(8,128)S(1)} %copy-done.5), kind=kOutput, calls=%fused_computation.2 | convolution fusion | flops 134807552 | bytes 5308416 | tf_op jit(solution)/shard_map/dot_general | solution.py:140
  264.9 12.0 %all-to-all-done.9 = bf16[8,16,4096]{2,1,0:T(8,128)(2,1)} async-done(((bf16[8,16,4096]{2,1,0:T(8,128)(2,1)}), bf16[8,16,4096]{2,1,0:T(8,128)(2,1)}, u32[]{:S(2)}, u32[]{:S(2)}) %all-to-all-start.9) | async-done | bytes 1048608 | tf_op jit(solution)/shard_map/all_to_all | solution.py:133
  276.9 2.3 convolution_add_fusion.1
  279.3 2.6 fusion
  (63 shorter events, 6.9 us)
Async XLA Ops:
  7.2 244.2 %copy-start = (bf16[1,1024,1024]{2,1,0:T(8,128)(2,1)S(1)}, bf16[1,1024,1024]{2,1,0:T(8,128)(2,1)}, u32[]{:S(2)}) copy-start(bf16[1,1024,1024]{2,1,0:T(8,128)(2,1)} %param.13) | copy-start | bytes 6291460
  7.2 101.4 %all-gather.12.cloned.1.call-start = ((), (), s32[]{:S(2)}) async-start(), calls=%async_computation.13 | async-start | bytes 10485760 | tf_op jit(solution)/shard_map/all_gather | solution.py:103
  7.9 2.2 copy-start.7
  10.1 6.0 %copy-start.8 = (s32[512,2]{0,1:T(2,128)S(1)}, s32[512,2]{0,1:T(2,128)}, u32[]{:S(2)}) copy-start(s32[512,2]{0,1:T(2,128)} %param.17) | copy-start | bytes 12292
  11.6 37.0 %copy-start.4 = (bf16[128,4096]{1,0:T(8,128)(2,1)S(1)}, bf16[128,4096]{1,0:T(8,128)(2,1)}, u32[]{:S(2)}) copy-start(bf16[128,4096]{1,0:T(8,128)(2,1)} %param.15) | copy-start | bytes 3145732
  11.6 27.6 %all-to-all-start = ((bf16[128,4,1024]{0,2,1:T(8,128)(2,1)}), bf16[128,4,1024]{0,2,1:T(8,128)(2,1)}, u32[]{:S(2)}, u32[]{:S(2)}) async-start(bf16[128,4,1024]{0,2,1:T(8,128)(2,1)} %bitcast.115), calls=%async_computation | async-start | bytes 2097152 | tf_op jit(solution)/shard_map/all_to_all | solution.py:50
  16.0 32.9 %copy-start.6 = (f32[4096]{0:T(1024)S(1)}, f32[4096]{0:T(1024)}, u32[]{:S(2)}) copy-start(f32[4096]{0:T(1024)} %param.16) | copy-start | bytes 49156
  16.0 122.0 %all-gather.6.cloned.1.call-start = ((), (), s32[]{:S(2)}) async-start(), calls=%async_computation.10 | async-start | bytes 5242880 | tf_op jit(solution)/shard_map/all_gather | solution.py:122
  42.3 6.3 %collective-permute-start = (bf16[16,1024]{1,0:T(8,128)(2,1)S(1)}, bf16[16,1024]{1,0:T(8,128)(2,1)}, u32[]{:S(2)}, u32[]{:S(2)}) collective-permute-start(bf16[16,1024]{1,0:T(8,128)(2,1)S(1)} %slice.56), channel_id=1, source_target_pairs={{0,4},{4,8},{8,12},{12,16},{16,20},{20,24},{24,28},{1,5},{5,9},{9,... | collective-permute-start | bytes 98312 | tf_op jit(solution)/shard_map/ppermute | solution.py:17
  79.9 79.0 %all-gather.8.cloned.1.call-start = ((), (), s32[]{:S(2)}) async-start(), calls=%async_computation.11 | async-start | bytes 5242880 | tf_op jit(solution)/shard_map/all_gather | solution.py:122
  108.6 82.5 %all-gather.10.cloned.1.call-start = ((), (), s32[]{:S(2)}) async-start(), calls=%async_computation.12 | async-start | bytes 5242880 | tf_op jit(solution)/shard_map/all_gather | solution.py:122
  138.1 4.3 %copy-start.10 = (bf16[512,4096]{1,0:T(8,128)(2,1)S(1)}, bf16[512,4096]{1,0:T(8,128)(2,1)}, u32[]{:S(2)}) copy-start(bf16[512,4096]{1,0:T(8,128)(2,1)} %all-gather.6.cloned.1.call-done) | copy-start | bytes 12582916
  138.1 4.8 %copy-start.12 = (bf16[1,4096,256]{2,1,0:T(8,128)(2,1)S(1)}, bf16[1,4096,256]{2,1,0:T(8,128)(2,1)}, u32[]{:S(2)}) copy-start(bf16[1,4096,256]{2,1,0:T(8,128)(2,1)} %param.20) | copy-start | bytes 6291460
  158.8 5.4 %copy-start.11 = (bf16[512,4096]{1,0:T(8,128)(2,1)S(1)}, bf16[512,4096]{1,0:T(8,128)(2,1)}, u32[]{:S(2)}) copy-start(bf16[512,4096]{1,0:T(8,128)(2,1)} %all-gather.8.cloned.1.call-done) | copy-start | bytes 12582916
  158.8 6.1 %copy-start.13 = (bf16[1,4096,256]{2,1,0:T(8,128)(2,1)S(1)}, bf16[1,4096,256]{2,1,0:T(8,128)(2,1)}, u32[]{:S(2)}) copy-start(bf16[1,4096,256]{2,1,0:T(8,128)(2,1)} %param.20) | copy-start | bytes 6291460
  178.0 29.7 %all-to-all-start.4 = ((bf16[8,16,4096]{2,1,0:T(8,128)(2,1)}), bf16[8,16,4096]{2,1,0:T(8,128)(2,1)S(1)}, u32[]{:S(2)}, u32[]{:S(2)}) async-start(bf16[8,16,4096]{2,1,0:T(8,128)(2,1)} %bitcast.123), calls=%async_computation.4 | async-start | bytes 2097152 | tf_op jit(solution)/shard_map/all_to_all | solution.py:133
  191.1 4.3 %copy-start.9 = (bf16[512,4096]{1,0:T(8,128)(2,1)S(1)}, bf16[512,4096]{1,0:T(8,128)(2,1)}, u32[]{:S(2)}) copy-start(bf16[512,4096]{1,0:T(8,128)(2,1)} %all-gather.10.cloned.1.call-done) | copy-start | bytes 12582916
  191.1 4.7 %copy-start.14 = (bf16[1,4096,256]{2,1,0:T(8,128)(2,1)S(1)}, bf16[1,4096,256]{2,1,0:T(8,128)(2,1)}, u32[]{:S(2)}) copy-start(bf16[1,4096,256]{2,1,0:T(8,128)(2,1)} %param.20) | copy-start | bytes 6291460
  207.7 9.4 %all-to-all-start.8 = ((bf16[4,128,256]{1,2,0:T(8,128)(2,1)}), bf16[4,128,256]{1,2,0:T(8,128)(2,1)S(1)}, u32[]{:S(2)}, u32[]{:S(2)}) async-start(bf16[4,128,256]{1,2,0:T(8,128)(2,1)} %copy.43), calls=%async_computation.8 | async-start | bytes 524288 | tf_op jit(solution)/shard_map/all_to_all | solution.py:131
  217.1 30.0 %all-to-all-start.6 = ((bf16[8,16,4096]{2,1,0:T(8,128)(2,1)}), bf16[8,16,4096]{2,1,0:T(8,128)(2,1)}, u32[]{:S(2)}, u32[]{:S(2)}) async-start(bf16[8,16,4096]{2,1,0:T(8,128)(2,1)} %bitcast.122), calls=%async_computation.6 | async-start | bytes 2097152 | tf_op jit(solution)/shard_map/all_to_all | solution.py:133
  224.1 1.4 copy-start.1
  224.1 5.9 %slice-start = ((s8[8388608]{0:T(1024)(128)(4,1)}), s8[4194304]{0:T(1024)(128)(4,1)S(1)}, s32[]{:S(2)}) async-start(s8[8388608]{0:T(1024)(128)(4,1)} %bitcast.108), calls=%async_computation.14 | async-start | bytes 8388608
  225.5 1.3 copy-start.2
  225.5 5.9 %slice-start.1 = ((s8[8388608]{0:T(1024)(128)(4,1)}), s8[4194304]{0:T(1024)(128)(4,1)S(1)}, s32[]{:S(2)}) async-start(s8[8388608]{0:T(1024)(128)(4,1)} %bitcast.108), calls=%async_computation.15 | async-start | bytes 8388608
  226.8 3.2 %copy-start.3 = (f32[521,1024]{1,0:T(8,128)}, f32[521,1024]{1,0:T(8,128)S(1)}, u32[]{:S(2)}) copy-start(f32[521,1024]{1,0:T(8,128)S(1)} %slice_add_fusion) | copy-start | bytes 6402052
  233.6 17.7 %copy-start.15 = (f32[1,1024]{1,0:T(1,128)S(1)}, f32[1,1024]{1,0:T(1,128)}, u32[]{:S(2)}) copy-start(f32[1,1024]{1,0:T(1,128)} %param.14) | copy-start | bytes 12292
  247.1 29.8 %all-to-all-start.9 = ((bf16[8,16,4096]{2,1,0:T(8,128)(2,1)}), bf16[8,16,4096]{2,1,0:T(8,128)(2,1)}, u32[]{:S(2)}, u32[]{:S(2)}) async-start(bf16[8,16,4096]{2,1,0:T(8,128)(2,1)} %bitcast.124), calls=%async_computation.9 | async-start | bytes 2097152 | tf_op jit(solution)/shard_map/all_to_all | solution.py:133
  259.5 0.8 copy-start.5
Sparse Core Ops, SparseCore 0:
  9.5 68.2 all-gather.11
  80.0 34.9 all-gather.5
  116.5 34.4 all-gather.7
  152.4 38.6 all-gather.9
